TPU v7x, 32 devices: a whole 2x2x4 slice. The times are simulated.
32 devices in a mesh: ep: 8 (over z, core), tp: 4 (over y, x).
Axes of the slice: x: 2, y: 2, z: 4, core: 2. Of those that a mesh axis runs over, the one named last changes fastest.
Arguments:
- tokens: bfloat16 [64, 2048], P('ep'), may hold values from -6 to 6
- attn_gain: float32 [2048], replicated, may hold values from 0.1 to 1.9
- query_weight: bfloat16 [2048, 4096], P('ep', 'tp'), may hold values from -0.125 to 0.125
- key_weight: bfloat16 [2048, 4096], P('ep', 'tp'), may hold values from -0.125 to 0.125
- value_weight: bfloat16 [2048, 4096], P('ep', 'tp'), may hold values from -0.125 to 0.125
- query_gain: float32 [128], replicated, may hold values from 0.1 to 1.9
- stick_bias: float32 [32], P('tp'), may hold values from -7 to -2.5
- key_cache: bfloat16 [64, 32, 512, 128], P('ep', 'tp'), may hold values from -6 to 6
- value_cache: bfloat16 [64, 32, 512, 128], P('ep', 'tp'), may hold values from -6 to 6
- lengths: int32 [64], P('ep'), may hold values from 64 to 512, as said below
- out_weight: bfloat16 [4096, 2048], P('tp'), may hold values from -0.375 to 0.375
- mix_gain: float32 [2048], replicated, may hold values from 0.1 to 1.9
- route_ids: int32 [64, 2], P('ep'), may hold values from 0 to 7, all different within a row; in each aligned block of 8 rows (0 to 7, 8 to 15, ...) at most 4 rows name the same one
- route_weights: float32 [64, 2], P('ep'), may hold values from 0.2 to 1
- expert_gate: bfloat16 [8, 2048, 2560], P('ep', None, 'tp'), may hold values from -0.125 to 0.125
- expert_up: bfloat16 [8, 2048, 2560], P('ep', None, 'tp'), may hold values from -0.125 to 0.125
- expert_down: bfloat16 [8, 2560, 2048], P('ep', 'tp'), may hold values from -0.15625 to 0.15625
- side_gate: bfloat16 [2048, 1024], P(None, 'tp'), may hold values from -0.125 to 0.125
- side_up: bfloat16 [2048, 1024], P(None, 'tp'), may hold values from -0.125 to 0.125
- side_down: bfloat16 [1024, 2048], P('tp'), may hold values from -0.25 to 0.25
- branch_gate: float32 [2048], replicated, may hold values from -0.125 to 0.125
Outputs:
- mixed: bfloat16 [64, 2048], P('ep', 'tp')
- new_keys: bfloat16 [64, 4096], P('ep', 'tp')
- new_values: bfloat16 [64, 4096], P('ep', 'tp')
Inputs may be any that keep to these rules, and one draw needn't show every extreme that they name: `lengths`: at least an eighth of 512; the first sequence has 512. `route_ids`: each token names 2 different experts. In the rows of one device no expert is named by more than 4 rows, a bound that some block reaches of some device.
All inputs are finite; a program needn't handle non-finite values.
Results may differ from a plain program's by a relative error of at most 0.018.
Values may be sent and summed in bfloat16 or wider, within the bound.
No kernel may reach another device: no remote copies, remote signals or barrier semaphores. Data moves between devices by JAX's collectives and lax.ppermute only.
A program may use at most 64 MiB of HBM per device.

v0:
```python
import jax
import jax.numpy as jnp
from jax import lax
from jax.sharding import PartitionSpec as P

DH = 128
epsilon = 1e-06


def rms_scale(values, scale_gain):
    mean_square = jnp.mean(values * values, axis=-1, keepdims=True)
    return values * lax.rsqrt(mean_square + epsilon) * scale_gain


def summed_blocks(partial, axis_name):
    count = lax.axis_size(axis_name)
    rows = partial.shape[0] // count
    blocks = lax.all_to_all(
        partial.astype(jnp.bfloat16), axis_name, split_axis=0, concat_axis=0, tiled=True
    )
    return jnp.sum(blocks.reshape(count, rows, -1).astype(jnp.float32), axis=0)


def body(
    tokens,
    attn_gain,
    query_weight,
    key_weight,
    value_weight,
    query_gain,
    stick_bias,
    key_cache,
    value_cache,
    lengths,
    out_weight,
    mix_gain,
    route_ids,
    route_weights,
    expert_gate,
    expert_up,
    expert_down,
    side_gate,
    side_up,
    side_down,
    branch_gate,
):
    seq_count, model_width = tokens.shape
    head_cols = query_weight.shape[1]
    heads_local = key_cache.shape[1]
    cache_slots = key_cache.shape[2]
    experts = lax.axis_size("ep")
    tp_size = lax.axis_size("tp")
    stream = tokens.astype(jnp.float32)
    normed = rms_scale(stream, attn_gain).astype(jnp.bfloat16)
    columns = lax.all_to_all(normed, "ep", split_axis=1, concat_axis=0, tiled=True)
    query_rows = summed_blocks(
        jnp.dot(columns, query_weight, preferred_element_type=jnp.float32), "ep"
    ).astype(jnp.bfloat16)
    query_heads = rms_scale(
        query_rows.astype(jnp.float32).reshape(seq_count, heads_local, DH), query_gain
    ).astype(jnp.bfloat16)
    fresh = jnp.concatenate(
        [
            jnp.dot(columns, key_weight, preferred_element_type=jnp.float32),
            jnp.dot(columns, value_weight, preferred_element_type=jnp.float32),
        ],
        axis=1,
    )
    fresh = summed_blocks(fresh, "ep").astype(jnp.bfloat16)
    new_values = fresh[:, head_cols:]
    new_keys = rms_scale(
        fresh[:, :head_cols].astype(jnp.float32).reshape(seq_count, heads_local, DH), 1.0
    )
    new_keys = new_keys.astype(jnp.bfloat16).reshape(seq_count, head_cols)
    scores = jnp.einsum("shd,shld->shl", query_heads, key_cache, preferred_element_type=jnp.float32)
    scores = scores * DH ** (-0.5) + stick_bias[None, :, None]
    positions = jnp.arange(cache_slots, dtype=jnp.int32)
    visible = positions[None, None, :] < lengths[:, None, None]
    log_rest = jnp.where(visible, jax.nn.log_sigmoid(-scores), 0.0)
    later = (positions[:, None] > positions[None, :]).astype(jnp.float32)
    log_between = jnp.dot(
        log_rest.reshape(-1, cache_slots), later, precision=lax.Precision.HIGHEST
    ).reshape(scores.shape)
    stick = jnp.where(visible, jnp.exp(jax.nn.log_sigmoid(scores) + log_between), 0.0).astype(
        jnp.bfloat16
    )
    attended = jnp.einsum("shl,shld->shd", stick, value_cache, preferred_element_type=jnp.float32)
    attended = attended.astype(jnp.bfloat16).reshape(seq_count, head_cols)
    attn_part = jnp.dot(attended, out_weight, preferred_element_type=jnp.float32)
    attn_parts = lax.all_gather(attn_part.astype(jnp.bfloat16), "tp", axis=0, tiled=False)
    attn_proj = jnp.sum(attn_parts.astype(jnp.float32), axis=0)
    middle = (stream + attn_proj).astype(jnp.bfloat16)
    normed_mix = rms_scale(middle.astype(jnp.float32), mix_gain).astype(jnp.bfloat16)
    top_count = route_ids.shape[1]
    capacity = max(2, 2 * top_count * seq_count // experts)
    slots = experts * capacity
    flat_ids = route_ids.reshape(-1)
    onehot = (flat_ids[:, None] == jnp.arange(experts, dtype=jnp.int32)[None, :]).astype(jnp.int32)
    order = jnp.arange(flat_ids.shape[0], dtype=jnp.int32)
    earlier = (order[:, None] > order[None, :]) & (flat_ids[:, None] == flat_ids[None, :])
    slot_index = jnp.sum(earlier.astype(jnp.int32), axis=1)
    target = flat_ids * capacity + slot_index
    route_map = (target[:, None] == jnp.arange(slots, dtype=jnp.int32)[None, :]).astype(
        jnp.bfloat16
    )
    dispatch = jnp.sum(route_map.reshape(seq_count, top_count, slots), axis=1).T
    outbox = jnp.dot(dispatch, normed_mix, preferred_element_type=jnp.float32).astype(jnp.bfloat16)
    slot_rows = lax.all_to_all(outbox, "ep", split_axis=0, concat_axis=0, tiled=True)
    side_gate_pre = jnp.dot(normed_mix, side_gate, preferred_element_type=jnp.float32)
    side_up_pre = jnp.dot(normed_mix, side_up, preferred_element_type=jnp.float32)
    side_hidden = (jax.nn.silu(side_gate_pre) * side_up_pre).astype(jnp.bfloat16)
    side_term = jnp.dot(side_hidden, side_down, preferred_element_type=jnp.float32)
    switch = jax.nn.sigmoid(
        jnp.sum(normed_mix.astype(jnp.float32) * branch_gate, axis=1, keepdims=True)
    )
    col_width = model_width // tp_size
    col_offset = lax.axis_index("tp") * col_width
    side_blocks = lax.all_to_all(
        side_term.astype(jnp.bfloat16).reshape(seq_count, tp_size, col_width).transpose(1, 0, 2),
        "tp",
        split_axis=0,
        concat_axis=0,
        tiled=True,
    )
    side_part = jnp.sum(side_blocks.astype(jnp.float32), axis=0)
    gate_pre = jnp.dot(slot_rows, expert_gate[0], preferred_element_type=jnp.float32)
    up_pre = jnp.dot(slot_rows, expert_up[0], preferred_element_type=jnp.float32)
    hidden = (jax.nn.silu(gate_pre) * up_pre).astype(jnp.bfloat16)
    expert_term = jnp.dot(hidden, expert_down[0], preferred_element_type=jnp.float32)
    expert_term = expert_term.astype(jnp.bfloat16).reshape(experts, capacity, tp_size, col_width)
    returned = lax.all_to_all(
        expert_term.transpose(0, 2, 1, 3).reshape(experts * tp_size, capacity, col_width),
        ("ep", "tp"),
        split_axis=0,
        concat_axis=0,
        tiled=True,
    )
    expert_out = jnp.sum(
        returned.reshape(experts, tp_size, capacity, col_width).astype(jnp.float32), axis=1
    ).astype(jnp.bfloat16)
    picked = jnp.dot(
        route_map, expert_out.reshape(slots, col_width), preferred_element_type=jnp.float32
    )
    routed = jnp.sum(
        route_weights[:, :, None] * picked.reshape(seq_count, top_count, col_width), axis=1
    )
    middle_cols = lax.dynamic_slice_in_dim(middle, col_offset, col_width, 1).astype(jnp.float32)
    mixed = (middle_cols + routed + switch * side_part).astype(jnp.bfloat16)
    return (mixed, new_keys, new_values)


def solution(mesh):
    in_specs = (
        P("ep", None),
        P(),
        P("ep", "tp"),
        P("ep", "tp"),
        P("ep", "tp"),
        P(),
        P("tp"),
        P("ep", "tp", None, None),
        P("ep", "tp", None, None),
        P("ep"),
        P("tp", None),
        P(),
        P("ep", None),
        P("ep", None),
        P("ep", None, "tp"),
        P("ep", None, "tp"),
        P("ep", "tp", None),
        P(None, "tp"),
        P(None, "tp"),
        P("tp", None),
        P(),
    )
    out_specs = (P("ep", "tp"), P("ep", "tp"), P("ep", "tp"))
    return jax.shard_map(body, mesh=mesh, in_specs=in_specs, out_specs=out_specs, check_vma=False)
```

profile of v0, /device:TPU:0, one launch (start us, length us, event | category | flops | bytes accessed | tf_op | source)
XLA Modules:
  0.0 91.9 jit_solution(14223555700688407675)
XLA Ops:
  0.6 0.0 copy-start
  0.6 0.0 copy-start.7
  0.7 1.0 %fusion.50 = f32[8]{0:T(128)S(1)} fusion(bf16[8,2048]{1,0:T(8,128)(2,1)} %param.21), kind=kLoop, calls=%fused_computation.61 | loop fusion | flops 49144 | bytes 32800 | tf_op jit(solution)/shard_map/reduce_sum | solution.py:11
  1.7 1.4 %fusion.52 = bf16[8,2048]{1,0:T(8,128)(2,1)} fusion(bf16[8,2048]{1,0:T(8,128)(2,1)} %param.21, f32[2048]{0:T(1024)} %param.22, f32[8]{0:T(128)S(1)} %add_rsqrt_fusion.3), kind=kLoop, calls=%fused_computation.63 | loop fusion | flops 65536 | bytes 73760 | tf_op jit(solution)/shard_map/convert_element_type | solution.py:54
  3.2 6.4 %all-to-all-start = ((bf16[8,8,256]{2,0,1:T(8,128)(2,1)}), bf16[8,8,256]{2,0,1:T(8,128)(2,1)S(1)}, u32[]{:S(2)}, u32[]{:S(2)}) async-start(bf16[8,8,256]{2,0,1:T(8,128)(2,1)} %bitcast), calls=%async_computation | async-start | bytes 65536 | tf_op jit(solution)/shard_map/all_to_all | solution.py:55
  9.5 0.7 iota_compare_fusion.1
  10.2 0.8 copy.31
  11.0 0.1 eq.51
  11.1 0.2 convert_reduce_fusion.2
  11.3 0.1 reduce_sum.136
  11.3 0.1 copy.33
  11.4 0.1 fusion.82
  11.5 3.7 %all-to-all-done = bf16[8,8,256]{2,0,1:T(8,128)(2,1)S(1)} async-done(((bf16[8,8,256]{2,0,1:T(8,128)(2,1)}), bf16[8,8,256]{2,0,1:T(8,128)(2,1)S(1)}, u32[]{:S(2)}, u32[]{:S(2)}) %all-to-all-start) | async-done | bytes 32800 | tf_op jit(solution)/shard_map/all_to_all | solution.py:55
  15.2 1.9 %fusion.9 = bf16[8,8,1024]{2,1,0:T(8,128)(2,1)} fusion(bf16[256,1024]{1,0:T(8,128)(2,1)} %param.23, bf16[8,8,256]{2,0,1:T(8,128)(2,1)S(1)} %all-to-all-done), kind=kOutput, calls=%fused_computation.13 | convolution fusion | flops 33619968 | bytes 688128 | tf_op jit(solution)/shard_map/dot_general | solution.py:57
  17.2 3.4 %all-to-all-start.1 = ((bf16[8,8,1024]{2,1,0:T(8,128)(2,1)}), bf16[8,8,1024]{2,1,0:T(8,128)(2,1)S(1)}, u32[]{:S(2)}, u32[]{:S(2)}) async-start(bf16[8,8,1024]{2,1,0:T(8,128)(2,1)} %fusion.9), calls=%async_computation.1 | async-start | bytes 262144 | tf_op jit(solution)/shard_map/all_to_all | solution.py:18
  20.5 1.3 %convolution_convert_fusion.3 = bf16[8,8,1024]{2,1,0:T(8,128)(2,1)S(1)} fusion(bf16[256,1024]{1,0:T(8,128)(2,1)} %param.25, bf16[8,8,256]{2,0,1:T(8,128)(2,1)S(1)} %all-to-all-done), kind=kOutput, calls=%fused_computation.10 | convolution fusion | flops 33619968 | bytes 688128 | tf_op jit(solution)/shard_map/dot_general | solution.py:65
  21.8 1.3 %convolution_convert_fusion.4 = bf16[8,8,1024]{2,1,0:T(8,128)(2,1)S(1)} fusion(bf16[256,1024]{1,0:T(8,128)(2,1)} %param.24, bf16[8,8,256]{2,0,1:T(8,128)(2,1)S(1)} %all-to-all-done), kind=kOutput, calls=%fused_computation.11 | convolution fusion | flops 33619968 | bytes 688128 | tf_op jit(solution)/shard_map/dot_general | solution.py:64
  23.1 0.7 pad_maximum_fusion
  23.8 3.5 %all-to-all-done.1 = bf16[8,8,1024]{2,1,0:T(8,128)(2,1)S(1)} async-done(((bf16[8,8,1024]{2,1,0:T(8,128)(2,1)}), bf16[8,8,1024]{2,1,0:T(8,128)(2,1)S(1)}, u32[]{:S(2)}, u32[]{:S(2)}) %all-to-all-start.1) | async-done | bytes 131104 | tf_op jit(solution)/shard_map/all_to_all | solution.py:18
  27.2 0.1 fusion.62
  27.3 0.0 copy-done.7
  27.3 0.1 fusion.70
  27.4 0.0 copy-start.9
  27.4 5.8 %fusion.68 = f32[8,8,1,512]{3,2,1,0:T(1,128)S(1)} fusion(bf16[8,8,512,128]{3,2,1,0:T(8,128)(2,1)} %param.28, bf16[8,8,128,1]{2,0,1,3:T(8,128)(2,1)S(1)} %fusion.70), kind=kOutput, calls=%fused_computation.85 | convolution fusion | flops 8388608 | bytes 8536064 | tf_op jit(solution)/shard_map/shd,shld->shl/dot_general | solution.py:75
  33.2 0.0 copy-done.9
  33.2 0.6 fusion.16
  33.8 0.0 copy-done.1
  33.8 0.0 copy-start.2
  33.8 1.2 %fusion.33 = f32[8,8,1,128]{3,2,1,0:T(1,128)S(1)} fusion(bf16[8,8,512,128]{3,2,1,0:T(8,128)(2,1)S(1)} %copy-done.1, bf16[8,8,512,1]{2,1,0,3:T(8,128)(2,1)S(1)} %fusion.16), kind=kOutput, calls=%fused_computation.39 | convolution fusion | flops 8388608 | bytes 8486912 | tf_op jit(solution)/shard_map/shl,shld->shd/dot_general | solution.py:87
  35.0 0.0 copy-start.3
  35.0 1.0 %copy-done.2 = bf16[1024,2048]{1,0:T(8,128)(2,1)S(1)} copy-done((bf16[1024,2048]{1,0:T(8,128)(2,1)S(1)}, bf16[1024,2048]{1,0:T(8,128)(2,1)}, u32[]{:S(2)}) %copy-start.2) | copy-done | bytes 4194328
  36.0 0.7 convolution_convert_fusion.2
  36.7 8.6 %all-gather = bf16[32,2048]{1,0:T(8,128)(2,1)S(1)} all-gather(bf16[8,2048]{1,0:T(8,128)(2,1)S(1)} %convolution_convert_fusion.2), channel_id=2, replica_groups=mesh['ep'=8,'tp'=4] {'tp'}, dimensions={0}, use_global_device_ids=true | all-gather | bytes 163840 | tf_op jit(solution)/shard_map/all_gather | solution.py:90
  45.3 0.0 copy-done.4
  45.3 0.1 fusion.47
  45.4 0.0 copy-done.5
  45.4 0.2 convolution_convert_fusion
  45.7 0.0 copy-done.3
  45.7 0.3 fusion.91
  46.0 2.9 %convolution_convert_fusion.1 = bf16[8,2048]{1,0:T(8,128)(2,1)} fusion(bf16[256,2048]{1,0:T(8,128)(2,1)} %param.40, bf16[2048,256]{1,0:T(8,128)(2,1)} %param.39, f32[8,256]{1,0:T(8,128)S(1)} %fusion.91, bf16[8,2048]{1,0:T(8,128)(2,1)S(1)} %get-tuple-element.4, f32[2048]{0:T(1024)S(1)} %copy-done.5, f32[8]{0:T(128)S(1)} %add_rsqrt_fusion.2), kind=kOutput, calls=%fused_computation.8 | convolution fusion | flops 16871424 | bytes 2179104 | tf_op jit(solution)/shard_map/dot_general | solution.py:112
  48.9 3.3 %all-to-all-start.4 = ((bf16[4,8,512]{2,1,0:T(8,128)(2,1)}), bf16[4,8,512]{2,1,0:T(8,128)(2,1)S(1)}, u32[]{:S(2)}, u32[]{:S(2)}) async-start(bf16[4,8,512]{2,1,0:T(8,128)(2,1)} %bitcast.21), calls=%async_computation.4 | async-start | bytes 65536 | tf_op jit(solution)/shard_map/all_to_all | solution.py:118
  52.2 0.0 copy-done.6
  52.2 0.2 multiply_reduce_fusion
  52.4 0.7 all_to_all.44
  53.1 3.8 %all-to-all-done.4 = bf16[4,8,512]{2,1,0:T(8,128)(2,1)S(1)} async-done(((bf16[4,8,512]{2,1,0:T(8,128)(2,1)}), bf16[4,8,512]{2,1,0:T(8,128)(2,1)S(1)}, u32[]{:S(2)}, u32[]{:S(2)}) %all-to-all-start.4) | async-done | bytes 32800 | tf_op jit(solution)/shard_map/all_to_all | solution.py:118
  56.9 3.4 %all-to-all-start.2 = ((bf16[8,4,2048]{2,1,0:T(4,128)(2,1)}), bf16[8,4,2048]{2,1,0:T(4,128)(2,1)S(1)}, u32[]{:S(2)}, u32[]{:S(2)}) async-start(bf16[8,4,2048]{2,1,0:T(4,128)(2,1)} %all_to_all.44), calls=%async_computation.2 | async-start | bytes 262144 | tf_op jit(solution)/shard_map/all_to_all | solution.py:108
  60.3 6.7 %all-to-all-done.2 = bf16[8,4,2048]{2,1,0:T(4,128)(2,1)S(1)} async-done(((bf16[8,4,2048]{2,1,0:T(4,128)(2,1)}), bf16[8,4,2048]{2,1,0:T(4,128)(2,1)S(1)}, u32[]{:S(2)}, u32[]{:S(2)}) %all-to-all-start.2) | async-done | bytes 131104 | tf_op jit(solution)/shard_map/all_to_all | solution.py:108
  66.9 3.4 %all-to-all-start.5 = ((bf16[8,8,2048]{2,1,0:T(8,128)(2,1)}), bf16[8,8,2048]{2,1,0:T(8,128)(2,1)S(1)}, u32[]{:S(2)}, u32[]{:S(2)}) async-start(bf16[8,8,2048]{2,1,0:T(8,128)(2,1)} %pad_maximum_fusion), calls=%async_computation.5 | async-start | bytes 524288 | tf_op jit(solution)/shard_map/all_to_all | solution.py:18
  70.4 2.3 %fusion.4 = f32[32,640]{1,0:T(8,128)S(1)} fusion(bf16[32,2048]{1,0:T(8,128)(2,1)S(1)} %all_to_all.46, bf16[1,2048,640]{2,1,0:T(8,128)(2,1)} %param.35), kind=kOutput, calls=%fused_computation.4 | convolution fusion | flops 83886080 | bytes 2834432 | tf_op jit(solution)/shard_map/dot_general | solution.py:126
  72.7 0.0 copy-done
  72.7 0.0 copy-start.8
  72.7 2.7 %fusion.6 = bf16[32,2048]{1,0:T(8,128)(2,1)S(1)} fusion(bf16[1,640,2048]{2,1,0:T(8,128)(2,1)S(1)} %copy-done, bf16[32,2048]{1,0:T(8,128)(2,1)S(1)} %all_to_all.46, bf16[1,2048,640]{2,1,0:T(8,128)(2,1)} %param.36, f32[32,640]{1,0:T(8,128)S(1)} %fusion.4), kind=kOutput, calls=%fused_computation.6 | convolution fusion | flops 167960576 | bytes 5586944 | tf_op jit(solution)/shard_map/dot_general | solution.py:129
  75.4 0.1 reshape.169
  75.5 0.7 copy.35
  76.2 3.8 %all-to-all-done.5 = bf16[8,8,2048]{2,1,0:T(8,128)(2,1)S(1)} async-done(((bf16[8,8,2048]{2,1,0:T(8,128)(2,1)}), bf16[8,8,2048]{2,1,0:T(8,128)(2,1)S(1)}, u32[]{:S(2)}, u32[]{:S(2)}) %all-to-all-start.5) | async-done | bytes 262176 | tf_op jit(solution)/shard_map/all_to_all | solution.py:18
  80.0 2.6 %all-to-all-start.3 = ((bf16[32,4,512]{2,1,0:T(4,128)(2,1)}), bf16[32,4,512]{2,1,0:T(4,128)(2,1)S(1)}, u32[]{:S(2)}, u32[]{:S(2)}) async-start(bf16[32,4,512]{2,1,0:T(4,128)(2,1)} %bitcast.18), calls=%async_computation.3 | async-start | bytes 262144 | tf_op jit(solution)/shard_map/all_to_all | solution.py:131
  82.6 0.1 fusion.60
  82.7 0.6 slice.9
  83.3 0.7 fusion.61
  84.0 6.9 %all-to-all-done.3 = bf16[32,4,512]{2,1,0:T(4,128)(2,1)S(1)} async-done(((bf16[32,4,512]{2,1,0:T(4,128)(2,1)}), bf16[32,4,512]{2,1,0:T(4,128)(2,1)S(1)}, u32[]{:S(2)}, u32[]{:S(2)}) %all-to-all-start.3) | async-done | bytes 131104 | tf_op jit(solution)/shard_map/all_to_all | solution.py:131
  91.0 0.1 bitcast_reduce_fusion
  91.0 0.0 copy-done.8
  91.0 0.2 fusion.20
  91.2 0.7 add_convert_fusion
  (17 shorter events, 0.2 us)
Async XLA Ops:
  0.6 72.0 %copy-start = (bf16[1,640,2048]{2,1,0:T(8,128)(2,1)S(1)}, bf16[1,640,2048]{2,1,0:T(8,128)(2,1)}, u32[]{:S(2)}) copy-start(bf16[1,640,2048]{2,1,0:T(8,128)(2,1)} %param.37) | copy-start | bytes 7864324
  0.6 26.7 %copy-start.7 = (f32[128]{0:T(128)S(1)}, f32[128]{0:T(128)}, u32[]{:S(2)}) copy-start(f32[128]{0:T(128)} %param.26) | copy-start | bytes 1540
  3.2 12.1 %all-to-all-start = ((bf16[8,8,256]{2,0,1:T(8,128)(2,1)}), bf16[8,8,256]{2,0,1:T(8,128)(2,1)S(1)}, u32[]{:S(2)}, u32[]{:S(2)}) async-start(bf16[8,8,256]{2,0,1:T(8,128)(2,1)} %bitcast), calls=%async_computation | async-start | bytes 65536 | tf_op jit(solution)/shard_map/all_to_all | solution.py:55
  17.2 10.1 %all-to-all-start.1 = ((bf16[8,8,1024]{2,1,0:T(8,128)(2,1)}), bf16[8,8,1024]{2,1,0:T(8,128)(2,1)S(1)}, u32[]{:S(2)}, u32[]{:S(2)}) async-start(bf16[8,8,1024]{2,1,0:T(8,128)(2,1)} %fusion.9), calls=%async_computation.1 | async-start | bytes 262144 | tf_op jit(solution)/shard_map/all_to_all | solution.py:18
  27.4 5.8 %copy-start.9 = (f32[8]{0:T(128)S(1)}, f32[8]{0:T(128)}, u32[]{:S(2)}) copy-start(f32[8]{0:T(128)} %param.27) | copy-start | bytes 100
  27.4 6.4 %copy-start.1 = (bf16[8,8,512,128]{3,2,1,0:T(8,128)(2,1)S(1)}, bf16[8,8,512,128]{3,2,1,0:T(8,128)(2,1)}, u32[]{:S(2)}) copy-start(bf16[8,8,512,128]{3,2,1,0:T(8,128)(2,1)} %param.29) | copy-start | bytes 25165828
  33.8 2.2 %copy-start.2 = (bf16[1024,2048]{1,0:T(8,128)(2,1)S(1)}, bf16[1024,2048]{1,0:T(8,128)(2,1)}, u32[]{:S(2)}) copy-start(bf16[1024,2048]{1,0:T(8,128)(2,1)} %param.31) | copy-start | bytes 12582916
  35.0 10.3 %copy-start.4 = (bf16[8,2048]{1,0:T(8,128)(2,1)S(1)}, bf16[8,2048]{1,0:T(8,128)(2,1)}, u32[]{:S(2)}) copy-start(bf16[8,2048]{1,0:T(8,128)(2,1)} %param.21) | copy-start | bytes 98308
  35.0 10.4 %copy-start.5 = (f32[2048]{0:T(1024)S(1)}, f32[2048]{0:T(1024)}, u32[]{:S(2)}) copy-start(f32[2048]{0:T(1024)} %param.32) | copy-start | bytes 24580
  35.0 10.7 %copy-start.3 = (bf16[2048,256]{1,0:T(8,128)(2,1)S(1)}, bf16[2048,256]{1,0:T(8,128)(2,1)}, u32[]{:S(2)}) copy-start(bf16[2048,256]{1,0:T(8,128)(2,1)} %param.38) | copy-start | bytes 3145732
  36.7 15.5 %copy-start.6 = (f32[2048]{0:T(1024)S(1)}, f32[2048]{0:T(1024)}, u32[]{:S(2)}) copy-start(f32[2048]{0:T(1024)} %param.41) | copy-start | bytes 24580
  48.9 8.0 %all-to-all-start.4 = ((bf16[4,8,512]{2,1,0:T(8,128)(2,1)}), bf16[4,8,512]{2,1,0:T(8,128)(2,1)S(1)}, u32[]{:S(2)}, u32[]{:S(2)}) async-start(bf16[4,8,512]{2,1,0:T(8,128)(2,1)} %bitcast.21), calls=%async_computation.4 | async-start | bytes 65536 | tf_op jit(solution)/shard_map/all_to_all | solution.py:118
  56.9 10.1 %all-to-all-start.2 = ((bf16[8,4,2048]{2,1,0:T(4,128)(2,1)}), bf16[8,4,2048]{2,1,0:T(4,128)(2,1)S(1)}, u32[]{:S(2)}, u32[]{:S(2)}) async-start(bf16[8,4,2048]{2,1,0:T(4,128)(2,1)} %all_to_all.44), calls=%async_computation.2 | async-start | bytes 262144 | tf_op jit(solution)/shard_map/all_to_all | solution.py:108
  66.9 13.1 %all-to-all-start.5 = ((bf16[8,8,2048]{2,1,0:T(8,128)(2,1)}), bf16[8,8,2048]{2,1,0:T(8,128)(2,1)S(1)}, u32[]{:S(2)}, u32[]{:S(2)}) async-start(bf16[8,8,2048]{2,1,0:T(8,128)(2,1)} %pad_maximum_fusion), calls=%async_computation.5 | async-start | bytes 524288 | tf_op jit(solution)/shard_map/all_to_all | solution.py:18
  72.7 18.4 %copy-start.8 = (f32[8,2]{0,1:T(2,128)S(1)}, f32[8,2]{0,1:T(2,128)}, u32[]{:S(2)}) copy-start(f32[8,2]{0,1:T(2,128)} %param.34) | copy-start | bytes 196
  80.0 10.9 %all-to-all-start.3 = ((bf16[32,4,512]{2,1,0:T(4,128)(2,1)}), bf16[32,4,512]{2,1,0:T(4,128)(2,1)S(1)}, u32[]{:S(2)}, u32[]{:S(2)}) async-start(bf16[32,4,512]{2,1,0:T(4,128)(2,1)} %bitcast.18), calls=%async_computation.3 | async-start | bytes 262144 | tf_op jit(solution)/shard_map/all_to_all | solution.py:131
where the time goes:
time: 92.9 us; the launch traced here: 91.9 us
  waiting for transfers between devices  28.4 us (31%)
  starting transfers between devices  22.3 us (24%)
  matrix products  21.2 us (23%)
  blocking collectives  8.59 us (9%)
  other arithmetic  6.32 us (7%)
  local copies, waits for them, and re-layouts  4.18 us (4%)
    all_gather x1, blocking collectives, body(): lax.all_gather(attn_part.astype(jnp.bfloat16), 'tp', axis=0, tiled=False)  8.59 us
    all_to_all x2, waiting for transfers between devices, summed_blocks(): lax.all_to_all(partial.astype(jnp.bfloat16), axis_name, split_axis=0, con...  7.22 us
    all_to_all x1, waiting for transfers between devices, body(): lax.all_to_all(expert_term.transpose(0, 2, 1, 3).reshape(experts * tp_siz...  6.94 us
    all_to_all x2, starting transfers between devices, summed_blocks(): lax.all_to_all(partial.astype(jnp.bfloat16), axis_name, split_axis=0, con...  6.78 us
    all_to_all x1, waiting for transfers between devices, body(): lax.all_to_all(outbox, 'ep', split_axis=0, concat_axis=0, tiled=True)  6.65 us
    all_to_all x1, starting transfers between devices, body(): lax.all_to_all(normed, 'ep', split_axis=1, concat_axis=0, tiled=True)  6.35 us
    dot_general x1, matrix products, body(): jnp.einsum('shd,shld->shl', query_heads, key_cache, preferred_element_typ...  5.79 us
    all_to_all x1, waiting for transfers between devices, body(): lax.all_to_all(side_term.astype(jnp.bfloat16).reshape(seq_count, tp_size,...  3.8 us
  transfers between devices with their start and end apart: 6, of which 6 were waited for; matrix products, arithmetic and copies ran while one was open for 14% of the time, Pallas kernels for 0%

commit v1 on v0

--- a/solution.py
+++ b/solution.py
@@ -52,7 +52,10 @@
     tp_size = lax.axis_size("tp")
     stream = tokens.astype(jnp.float32)
     normed = rms_scale(stream, attn_gain).astype(jnp.bfloat16)
-    columns = lax.all_to_all(normed, "ep", split_axis=1, concat_axis=0, tiled=True)
+    columns = jnp.concatenate(
+        lax.all_to_all(jnp.stack(jnp.split(normed, lax.axis_size("ep"), axis=1)), "ep", 0, 0),
+        axis=0,
+    )
     query_rows = summed_blocks(
         jnp.dot(columns, query_weight, preferred_element_type=jnp.float32), "ep"
     ).astype(jnp.bfloat16)

time: 92.9 us -> 96.8 us (1.042)
  local copies, waits for them, and re-layouts: 4.18 us -> 8.91 us
    unnamed x21 -> x28, local copies, waits for them, and re-layouts: 1.76 us -> 5.9 us
  transfers between devices with their start and end apart: 6 -> 6, of which waited for: 6 -> 6; matrix products, arithmetic and copies ran while one was open for 14% -> 13% of each run, Pallas kernels for 0% -> 0%
where the time goes in v1:
time: 96.8 us; the launch traced here: 95.8 us
  waiting for transfers between devices  28.1 us (29%)
  starting transfers between devices  22.3 us (23%)
  matrix products  21.2 us (22%)
  local copies, waits for them, and re-layouts  8.91 us (9%)
  blocking collectives  8.59 us (9%)
  other arithmetic  5.72 us (6%)
    all_gather x1, blocking collectives, body(): lax.all_gather(attn_part.astype(jnp.bfloat16), 'tp', axis=0, tiled=False)  8.59 us
    all_to_all x2, waiting for transfers between devices, summed_blocks(): lax.all_to_all(partial.astype(jnp.bfloat16), axis_name, split_axis=0, con...  7.22 us
    all_to_all x1, waiting for transfers between devices, body(): lax.all_to_all(expert_term.transpose(0, 2, 1, 3).reshape(experts * tp_siz...  6.94 us
    all_to_all x2, starting transfers between devices, summed_blocks(): lax.all_to_all(partial.astype(jnp.bfloat16), axis_name, split_axis=0, con...  6.78 us
    all_to_all x1, waiting for transfers between devices, body(): lax.all_to_all(outbox, 'ep', split_axis=0, concat_axis=0, tiled=True)  6.65 us
    all_to_all x1, starting transfers between devices, body(): lax.all_to_all(jnp.stack(jnp.split(normed, lax.axis_size('ep'), axis=1)),...  6.35 us
    unnamed x28, local copies, waits for them, and re-layouts  5.9 us
    dot_general x1, matrix products, body(): jnp.einsum('shd,shld->shl', query_heads, key_cache, preferred_element_typ...  5.79 us
  transfers between devices with their start and end apart: 6, of which 6 were waited for; matrix products, arithmetic and copies ran while one was open for 13% of the time, Pallas kernels for 0%

profile of v1, /device:TPU:0, one launch (start us, length us, event | category | flops | bytes accessed | tf_op | source)
XLA Modules:
  0.0 95.8 jit_solution(17144845823048908760)
XLA Ops:
  0.6 0.0 copy-start
  0.6 0.0 copy-start.7
  0.7 1.0 %fusion.50 = f32[8]{0:T(128)S(1)} fusion(bf16[8,2048]{1,0:T(8,128)(2,1)} %param.21), kind=kLoop, calls=%fused_computation.61 | loop fusion | flops 49144 | bytes 32800 | tf_op jit(solution)/shard_map/reduce_sum | solution.py:11
  1.7 0.8 fusion.52
  2.6 0.6 constant_dynamic-update-slice_fusion.7
  3.1 0.6 constant_dynamic-update-slice_fusion.6
  3.7 0.6 constant_dynamic-update-slice_fusion.5
  4.3 0.6 constant_dynamic-update-slice_fusion.4
  4.9 0.6 constant_dynamic-update-slice_fusion.3
  5.5 0.6 constant_dynamic-update-slice_fusion.2
  6.1 0.6 constant_dynamic-update-slice_fusion.1
  6.7 0.6 constant_dynamic-update-slice_fusion
  7.3 6.4 %all-to-all-start = ((bf16[8,8,256]{2,1,0:T(8,128)(2,1)}), bf16[8,8,256]{2,1,0:T(8,128)(2,1)S(1)}, u32[]{:S(2)}, u32[]{:S(2)}) async-start(bf16[8,8,256]{2,1,0:T(8,128)(2,1)} %constant_dynamic-update-slice_fusion), calls=%async_computation | async-start | bytes 65536 | tf_op jit(solution)/shard_map/all_to_all | solution.py:56
  13.6 0.7 iota_compare_fusion.1
  14.4 0.8 copy.31
  15.1 0.1 eq.51
  15.2 0.2 convert_reduce_fusion.2
  15.4 0.1 reduce_sum.136
  15.5 0.1 copy.33
  15.6 0.1 fusion.80
  15.6 3.7 %all-to-all-done = bf16[8,8,256]{2,1,0:T(8,128)(2,1)S(1)} async-done(((bf16[8,8,256]{2,1,0:T(8,128)(2,1)}), bf16[8,8,256]{2,1,0:T(8,128)(2,1)S(1)}, u32[]{:S(2)}, u32[]{:S(2)}) %all-to-all-start) | async-done | bytes 32800 | tf_op jit(solution)/shard_map/all_to_all | solution.py:56
  19.4 1.9 %fusion.9 = bf16[8,8,1024]{2,1,0:T(8,128)(2,1)} fusion(bf16[256,1024]{1,0:T(8,128)(2,1)} %param.23, bf16[8,8,256]{2,1,0:T(8,128)(2,1)S(1)} %all-to-all-done), kind=kOutput, calls=%fused_computation.13 | convolution fusion | flops 33619968 | bytes 688128 | tf_op jit(solution)/shard_map/dot_general | solution.py:60
  21.3 3.4 %all-to-all-start.1 = ((bf16[8,8,1024]{2,1,0:T(8,128)(2,1)}), bf16[8,8,1024]{2,1,0:T(8,128)(2,1)S(1)}, u32[]{:S(2)}, u32[]{:S(2)}) async-start(bf16[8,8,1024]{2,1,0:T(8,128)(2,1)} %fusion.9), calls=%async_computation.1 | async-start | bytes 262144 | tf_op jit(solution)/shard_map/all_to_all | solution.py:18
  24.7 1.3 %convolution_convert_fusion.3 = bf16[8,8,1024]{2,1,0:T(8,128)(2,1)S(1)} fusion(bf16[8,8,256]{2,1,0:T(8,128)(2,1)S(1)} %all-to-all-done, bf16[256,1024]{1,0:T(8,128)(2,1)} %param.25), kind=kOutput, calls=%fused_computation.10 | convolution fusion | flops 33619968 | bytes 688128 | tf_op jit(solution)/shard_map/dot_general | solution.py:68
  25.9 1.3 %convolution_convert_fusion.4 = bf16[8,8,1024]{2,1,0:T(8,128)(2,1)S(1)} fusion(bf16[8,8,256]{2,1,0:T(8,128)(2,1)S(1)} %all-to-all-done, bf16[256,1024]{1,0:T(8,128)(2,1)} %param.24), kind=kOutput, calls=%fused_computation.11 | convolution fusion | flops 33619968 | bytes 688128 | tf_op jit(solution)/shard_map/dot_general | solution.py:67
  27.2 0.7 pad_maximum_fusion
  27.9 3.5 %all-to-all-done.1 = bf16[8,8,1024]{2,1,0:T(8,128)(2,1)S(1)} async-done(((bf16[8,8,1024]{2,1,0:T(8,128)(2,1)}), bf16[8,8,1024]{2,1,0:T(8,128)(2,1)S(1)}, u32[]{:S(2)}, u32[]{:S(2)}) %all-to-all-start.1) | async-done | bytes 131104 | tf_op jit(solution)/shard_map/all_to_all | solution.py:18
  31.4 0.1 fusion.62
  31.5 0.0 copy-done.7
  31.5 0.1 fusion.68
  31.6 5.8 %fusion.66 = f32[8,8,1,512]{3,2,1,0:T(1,128)S(1)} fusion(bf16[8,8,512,128]{3,2,1,0:T(8,128)(2,1)} %param.28, bf16[8,8,128,1]{2,0,1,3:T(8,128)(2,1)S(1)} %fusion.68), kind=kOutput, calls=%fused_computation.83 | convolution fusion | flops 8388608 | bytes 8536064 | tf_op jit(solution)/shard_map/shd,shld->shl/dot_general | solution.py:78
  37.4 0.0 copy-done.9
  37.4 0.6 fusion.16
  37.9 0.0 copy-start.2
  38.0 1.2 %fusion.33 = f32[8,8,1,128]{3,2,1,0:T(1,128)S(1)} fusion(bf16[8,8,512,128]{3,2,1,0:T(8,128)(2,1)S(1)} %copy-done.1, bf16[8,8,512,1]{2,1,0,3:T(8,128)(2,1)S(1)} %fusion.16), kind=kOutput, calls=%fused_computation.39 | convolution fusion | flops 8388608 | bytes 8486912 | tf_op jit(solution)/shard_map/shl,shld->shd/dot_general | solution.py:90
  39.2 0.0 copy-start.5
  39.2 1.0 %copy-done.2 = bf16[1024,2048]{1,0:T(8,128)(2,1)S(1)} copy-done((bf16[1024,2048]{1,0:T(8,128)(2,1)S(1)}, bf16[1024,2048]{1,0:T(8,128)(2,1)}, u32[]{:S(2)}) %copy-start.2) | copy-done | bytes 4194328
  40.1 0.7 convolution_convert_fusion.2
  40.8 8.6 %all-gather = bf16[32,2048]{1,0:T(8,128)(2,1)S(1)} all-gather(bf16[8,2048]{1,0:T(8,128)(2,1)S(1)} %convolution_convert_fusion.2), channel_id=2, replica_groups=mesh['ep'=8,'tp'=4] {'tp'}, dimensions={0}, use_global_device_ids=true | all-gather | bytes 163840 | tf_op jit(solution)/shard_map/all_gather | solution.py:93
  49.4 0.1 fusion.47
  49.6 0.3 fusion.89
  49.9 2.9 %convolution_convert_fusion.1 = bf16[8,2048]{1,0:T(8,128)(2,1)} fusion(bf16[256,2048]{1,0:T(8,128)(2,1)} %param.40, bf16[2048,256]{1,0:T(8,128)(2,1)} %param.39, f32[8,256]{1,0:T(8,128)S(1)} %fusion.89, bf16[8,2048]{1,0:T(8,128)(2,1)S(1)} %get-tuple-element.4, f32[2048]{0:T(1024)S(1)} %copy-done.5, f32[8]{0:T(128)S(1)} %add_rsqrt_fusion.2), kind=kOutput, calls=%fused_computation.8 | convolution fusion | flops 16871424 | bytes 2179104 | tf_op jit(solution)/shard_map/dot_general | solution.py:115
  52.8 3.3 %all-to-all-start.4 = ((bf16[4,8,512]{2,1,0:T(8,128)(2,1)}), bf16[4,8,512]{2,1,0:T(8,128)(2,1)S(1)}, u32[]{:S(2)}, u32[]{:S(2)}) async-start(bf16[4,8,512]{2,1,0:T(8,128)(2,1)} %bitcast.27), calls=%async_computation.4 | async-start | bytes 65536 | tf_op jit(solution)/shard_map/all_to_all | solution.py:121
  56.0 0.2 convolution_convert_fusion
  56.3 0.2 multiply_reduce_fusion
  56.5 0.7 all_to_all.30
  57.2 3.6 %all-to-all-done.4 = bf16[4,8,512]{2,1,0:T(8,128)(2,1)S(1)} async-done(((bf16[4,8,512]{2,1,0:T(8,128)(2,1)}), bf16[4,8,512]{2,1,0:T(8,128)(2,1)S(1)}, u32[]{:S(2)}, u32[]{:S(2)}) %all-to-all-start.4) | async-done | bytes 32800 | tf_op jit(solution)/shard_map/all_to_all | solution.py:121
  60.8 3.4 %all-to-all-start.2 = ((bf16[8,4,2048]{2,1,0:T(4,128)(2,1)}), bf16[8,4,2048]{2,1,0:T(4,128)(2,1)S(1)}, u32[]{:S(2)}, u32[]{:S(2)}) async-start(bf16[8,4,2048]{2,1,0:T(4,128)(2,1)} %all_to_all.30), calls=%async_computation.2 | async-start | bytes 262144 | tf_op jit(solution)/shard_map/all_to_all | solution.py:111
  64.2 6.7 %all-to-all-done.2 = bf16[8,4,2048]{2,1,0:T(4,128)(2,1)S(1)} async-done(((bf16[8,4,2048]{2,1,0:T(4,128)(2,1)}), bf16[8,4,2048]{2,1,0:T(4,128)(2,1)S(1)}, u32[]{:S(2)}, u32[]{:S(2)}) %all-to-all-start.2) | async-done | bytes 131104 | tf_op jit(solution)/shard_map/all_to_all | solution.py:111
  70.8 3.4 %all-to-all-start.5 = ((bf16[8,8,2048]{2,1,0:T(8,128)(2,1)}), bf16[8,8,2048]{2,1,0:T(8,128)(2,1)S(1)}, u32[]{:S(2)}, u32[]{:S(2)}) async-start(bf16[8,8,2048]{2,1,0:T(8,128)(2,1)} %pad_maximum_fusion), calls=%async_computation.5 | async-start | bytes 524288 | tf_op jit(solution)/shard_map/all_to_all | solution.py:18
  74.3 2.3 %fusion.4 = f32[32,640]{1,0:T(8,128)S(1)} fusion(bf16[32,2048]{1,0:T(8,128)(2,1)S(1)} %all_to_all.32, bf16[1,2048,640]{2,1,0:T(8,128)(2,1)} %param.35), kind=kOutput, calls=%fused_computation.4 | convolution fusion | flops 83886080 | bytes 2834432 | tf_op jit(solution)/shard_map/dot_general | solution.py:129
  76.6 0.0 copy-start.8
  76.6 2.7 %fusion.6 = bf16[32,2048]{1,0:T(8,128)(2,1)S(1)} fusion(bf16[1,640,2048]{2,1,0:T(8,128)(2,1)S(1)} %copy-done, bf16[32,2048]{1,0:T(8,128)(2,1)S(1)} %all_to_all.32, bf16[1,2048,640]{2,1,0:T(8,128)(2,1)} %param.36, f32[32,640]{1,0:T(8,128)S(1)} %fusion.4), kind=kOutput, calls=%fused_computation.6 | convolution fusion | flops 167960576 | bytes 5586944 | tf_op jit(solution)/shard_map/dot_general | solution.py:132
  79.3 0.1 reshape.170
  79.4 0.7 copy.35
  80.1 3.8 %all-to-all-done.5 = bf16[8,8,2048]{2,1,0:T(8,128)(2,1)S(1)} async-done(((bf16[8,8,2048]{2,1,0:T(8,128)(2,1)}), bf16[8,8,2048]{2,1,0:T(8,128)(2,1)S(1)}, u32[]{:S(2)}, u32[]{:S(2)}) %all-to-all-start.5) | async-done | bytes 262176 | tf_op jit(solution)/shard_map/all_to_all | solution.py:18
  83.9 2.6 %all-to-all-start.3 = ((bf16[32,4,512]{2,1,0:T(4,128)(2,1)}), bf16[32,4,512]{2,1,0:T(4,128)(2,1)S(1)}, u32[]{:S(2)}, u32[]{:S(2)}) async-start(bf16[32,4,512]{2,1,0:T(4,128)(2,1)} %bitcast.24), calls=%async_computation.3 | async-start | bytes 262144 | tf_op jit(solution)/shard_map/all_to_all | solution.py:134
  86.5 0.1 fusion.60
  86.6 0.6 slice.9
  87.2 0.7 fusion.61
  87.9 6.9 %all-to-all-done.3 = bf16[32,4,512]{2,1,0:T(4,128)(2,1)S(1)} async-done(((bf16[32,4,512]{2,1,0:T(4,128)(2,1)}), bf16[32,4,512]{2,1,0:T(4,128)(2,1)S(1)}, u32[]{:S(2)}, u32[]{:S(2)}) %all-to-all-start.3) | async-done | bytes 131104 | tf_op jit(solution)/shard_map/all_to_all | solution.py:134
  94.8 0.1 bitcast_reduce_fusion
  94.9 0.2 fusion.20
  95.1 0.7 add_convert_fusion
  (25 shorter events, 0.2 us)
Async XLA Ops:
  0.6 75.9 %copy-start = (bf16[1,640,2048]{2,1,0:T(8,128)(2,1)S(1)}, bf16[1,640,2048]{2,1,0:T(8,128)(2,1)}, u32[]{:S(2)}) copy-start(bf16[1,640,2048]{2,1,0:T(8,128)(2,1)} %param.37) | copy-start | bytes 7864324
  0.6 30.8 %copy-start.7 = (f32[128]{0:T(128)S(1)}, f32[128]{0:T(128)}, u32[]{:S(2)}) copy-start(f32[128]{0:T(128)} %param.26) | copy-start | bytes 1540
  7.3 12.1 %all-to-all-start = ((bf16[8,8,256]{2,1,0:T(8,128)(2,1)}), bf16[8,8,256]{2,1,0:T(8,128)(2,1)S(1)}, u32[]{:S(2)}, u32[]{:S(2)}) async-start(bf16[8,8,256]{2,1,0:T(8,128)(2,1)} %constant_dynamic-update-slice_fusion), calls=%async_computation | async-start | bytes 65536 | tf_op jit(solution)/shard_map/all_to_all | solution.py:56
  21.3 10.1 %all-to-all-start.1 = ((bf16[8,8,1024]{2,1,0:T(8,128)(2,1)}), bf16[8,8,1024]{2,1,0:T(8,128)(2,1)S(1)}, u32[]{:S(2)}, u32[]{:S(2)}) async-start(bf16[8,8,1024]{2,1,0:T(8,128)(2,1)} %fusion.9), calls=%async_computation.1 | async-start | bytes 262144 | tf_op jit(solution)/shard_map/all_to_all | solution.py:18
  31.6 5.8 %copy-start.9 = (f32[8]{0:T(128)S(1)}, f32[8]{0:T(128)}, u32[]{:S(2)}) copy-start(f32[8]{0:T(128)} %param.27) | copy-start | bytes 100
  31.6 6.4 %copy-start.1 = (bf16[8,8,512,128]{3,2,1,0:T(8,128)(2,1)S(1)}, bf16[8,8,512,128]{3,2,1,0:T(8,128)(2,1)}, u32[]{:S(2)}) copy-start(bf16[8,8,512,128]{3,2,1,0:T(8,128)(2,1)} %param.29) | copy-start | bytes 25165828
  37.9 2.2 %copy-start.2 = (bf16[1024,2048]{1,0:T(8,128)(2,1)S(1)}, bf16[1024,2048]{1,0:T(8,128)(2,1)}, u32[]{:S(2)}) copy-start(bf16[1024,2048]{1,0:T(8,128)(2,1)} %param.31) | copy-start | bytes 12582916
  39.1 10.3 %copy-start.4 = (bf16[8,2048]{1,0:T(8,128)(2,1)S(1)}, bf16[8,2048]{1,0:T(8,128)(2,1)}, u32[]{:S(2)}) copy-start(bf16[8,2048]{1,0:T(8,128)(2,1)} %param.21) | copy-start | bytes 98308
  39.1 10.4 %copy-start.3 = (bf16[2048,256]{1,0:T(8,128)(2,1)S(1)}, bf16[2048,256]{1,0:T(8,128)(2,1)}, u32[]{:S(2)}) copy-start(bf16[2048,256]{1,0:T(8,128)(2,1)} %param.38) | copy-start | bytes 3145732
  39.2 10.4 %copy-start.5 = (f32[2048]{0:T(1024)S(1)}, f32[2048]{0:T(1024)}, u32[]{:S(2)}) copy-start(f32[2048]{0:T(1024)} %param.32) | copy-start | bytes 24580
  40.8 15.5 %copy-start.6 = (f32[2048]{0:T(1024)S(1)}, f32[2048]{0:T(1024)}, u32[]{:S(2)}) copy-start(f32[2048]{0:T(1024)} %param.41) | copy-start | bytes 24580
  52.8 8.0 %all-to-all-start.4 = ((bf16[4,8,512]{2,1,0:T(8,128)(2,1)}), bf16[4,8,512]{2,1,0:T(8,128)(2,1)S(1)}, u32[]{:S(2)}, u32[]{:S(2)}) async-start(bf16[4,8,512]{2,1,0:T(8,128)(2,1)} %bitcast.27), calls=%async_computation.4 | async-start | bytes 65536 | tf_op jit(solution)/shard_map/all_to_all | solution.py:121
  60.8 10.1 %all-to-all-start.2 = ((bf16[8,4,2048]{2,1,0:T(4,128)(2,1)}), bf16[8,4,2048]{2,1,0:T(4,128)(2,1)S(1)}, u32[]{:S(2)}, u32[]{:S(2)}) async-start(bf16[8,4,2048]{2,1,0:T(4,128)(2,1)} %all_to_all.30), calls=%async_computation.2 | async-start | bytes 262144 | tf_op jit(solution)/shard_map/all_to_all | solution.py:111
  70.8 13.1 %all-to-all-start.5 = ((bf16[8,8,2048]{2,1,0:T(8,128)(2,1)}), bf16[8,8,2048]{2,1,0:T(8,128)(2,1)S(1)}, u32[]{:S(2)}, u32[]{:S(2)}) async-start(bf16[8,8,2048]{2,1,0:T(8,128)(2,1)} %pad_maximum_fusion), calls=%async_computation.5 | async-start | bytes 524288 | tf_op jit(solution)/shard_map/all_to_all | solution.py:18
  76.6 18.4 %copy-start.8 = (f32[8,2]{0,1:T(2,128)S(1)}, f32[8,2]{0,1:T(2,128)}, u32[]{:S(2)}) copy-start(f32[8,2]{0,1:T(2,128)} %param.34) | copy-start | bytes 196
  83.9 10.9 %all-to-all-start.3 = ((bf16[32,4,512]{2,1,0:T(4,128)(2,1)}), bf16[32,4,512]{2,1,0:T(4,128)(2,1)S(1)}, u32[]{:S(2)}, u32[]{:S(2)}) async-start(bf16[32,4,512]{2,1,0:T(4,128)(2,1)} %bitcast.24), calls=%async_computation.3 | async-start | bytes 262144 | tf_op jit(solution)/shard_map/all_to_all | solution.py:134
